TPU v7x, 32 devices: a whole 2x2x4 slice. The times are simulated.
32 devices in a mesh: ep: 8 (over z, x), tp: 4 (over y, core).
Axes of the slice: x: 2, y: 2, z: 4, core: 2. Of those that a mesh axis runs over, the one named last changes fastest.
Arguments:
- mix_query: bfloat16 [2048, 2048], P('ep', 'tp'), may hold values from -6 to 6
- forget_input: bfloat16 [2048, 2048], P('ep', 'tp'), may hold values from -6 to 6
- mix_value: bfloat16 [2048, 2048], P('ep', 'tp'), may hold values from -6 to 6
- out_gate_input: bfloat16 [2048, 2048], P('ep', 'tp'), may hold values from -6 to 6
- decay_shift: float32 [2048, 16], P('ep', 'tp'), may hold values from -1.5 to 0
- forget_floor: float32 [2048], P('tp'), may hold values from 0.9 to 1
- head_gain: float32 [128], replicated, may hold values from 0.1 to 1.9
- w_mix_out: bfloat16 [2048, 2048], P(None, 'tp'), may hold values from -0.125 to 0.125
- moe_input: bfloat16 [2048, 2048], P('ep'), may hold values from -6 to 6
- moe_gain: float32 [2048], replicated, may hold values from 0.1 to 1.9
- routes: int32 [2048, 2], P('ep'), may hold values from 0 to 7, all different within a row; in each aligned block of 256 rows (0 to 255, 256 to 511, ...) at most 80 rows name the same one
- route_weight: float32 [2048, 2], P('ep'), may hold values from 0.1 to 1
- w_exp_gate: bfloat16 [8, 2048, 4096], P('ep', None, 'tp'), may hold values from -0.125 to 0.125
- w_exp_up: bfloat16 [8, 2048, 4096], P('ep', None, 'tp'), may hold values from -0.125 to 0.125
- w_exp_down: bfloat16 [8, 4096, 2048], P('ep', 'tp'), may hold values from -0.125 to 0.125
Outputs:
- mixed: bfloat16 [2048, 2048], P('ep', 'tp')
- moe_out: bfloat16 [2048, 2048], P('ep', 'tp')
Inputs may be any that keep to these rules, and one draw needn't show every extreme that they name: `routes`: at most 80 of the rows of one index of ep name one expert, and in every draw some device's rows name one expert exactly 80 times; the experts of a row differ.
All inputs are finite; a program needn't handle non-finite values.
Results may differ from a plain program's by a relative error of at most 0.02.
Values may be sent and summed in bfloat16 or wider, within the bound.
A program may use at most 64 MiB of HBM per device.

v0:
```python
import jax
import jax.numpy as jnp
from jax import lax
from jax.sharding import PartitionSpec as P

TOP_K = 2


eps = 1e-06
highest_precision = lax.Precision.HIGHEST


def carried_in(shard, axis, join, neutral):
    place = lax.axis_index(axis)
    gathered = jax.tree.map(
        lambda a, kind: lax.all_gather(a.astype(kind), axis), shard, (jnp.bfloat16, jnp.bfloat16)
    )
    state = jax.tree.map(lambda a, e: jnp.zeros_like(a) + jnp.asarray(e, a.dtype), shard, neutral)

    def one(turn, state):
        return join(
            state,
            jax.tree.map(
                lambda a, own: lax.dynamic_index_in_dim(a, turn, 0, False).astype(own.dtype),
                gathered,
                shard,
            ),
        )

    return lax.fori_loop(0, place, one, state)


def chain_step(earlier, later):
    return (earlier[0] * later[0], later[0][:, :, None] * earlier[1] + later[1])


def token_mixer(
    mix_query,
    forget_input,
    mix_value,
    out_gate_input,
    decay_shift,
    forget_floor,
    head_gain,
    w_mix_out,
):
    length = mix_query.shape[0]
    heads_here = decay_shift.shape[1]
    head_size = head_gain.shape[0]
    gate_input = forget_input.astype(jnp.float32)
    forget = forget_floor + (1.0 - forget_floor) * jax.nn.sigmoid(gate_input)
    input_gate = (1.0 - forget_floor) * jax.nn.sigmoid(-gate_input)
    log_decay = jnp.log(forget) + jnp.repeat(decay_shift, head_size, axis=1)

    def by_head(array):
        return array.reshape(length, heads_here, head_size).transpose(1, 0, 2)

    running_decay = jnp.cumsum(by_head(log_decay), axis=1)
    query_rows = by_head(mix_query.astype(jnp.float32)) * jnp.exp(running_decay)
    head_keys = by_head(input_gate)
    values = by_head(mix_value.astype(jnp.float32))
    scores = jnp.einsum(
        "htk,hsk->hts", query_rows, head_keys * jnp.exp(-running_decay), precision=highest_precision
    )
    causal = jnp.arange(length)[:, None] >= jnp.arange(length)[None, :]
    scores = jnp.where(causal[None, :, :], scores, 0.0)
    within_block_output = jnp.einsum("hts,hsv->htv", scores, values, precision=highest_precision)
    closing_total = running_decay[:, -1, :]
    carried_over_state = jnp.einsum(
        "gbx,gbi->gxi",
        head_keys * jnp.exp(closing_total[:, None, :] - running_decay),
        values,
        precision=highest_precision,
    )
    incoming_state = carried_in(
        (jnp.exp(closing_total), carried_over_state),
        "ep",
        chain_step,
        (jnp.ones_like(closing_total), jnp.zeros_like(carried_over_state)),
    )[1]
    block_result = within_block_output + jnp.einsum(
        "rsd,rda->rsa", query_rows, incoming_state, precision=highest_precision
    )
    inverse = lax.rsqrt(jnp.mean(block_result * block_result, axis=2, keepdims=True) + eps)
    gated = by_head(jax.nn.silu(out_gate_input.astype(jnp.float32)))
    normed_heads = (block_result * inverse * head_gain * gated).transpose(1, 0, 2)
    head_out = normed_heads.reshape(length, heads_here * head_size).astype(jnp.bfloat16)
    mixed = jnp.dot(
        lax.all_gather(head_out, "tp", axis=1, tiled=True),
        w_mix_out,
        preferred_element_type=jnp.float32,
    )
    return mixed.astype(jnp.bfloat16)


def experts_layer(moe_input, moe_gain, routes, route_weight, w_exp_gate, w_exp_up, w_exp_down):
    row_count = moe_input.shape[0]
    expert_count = lax.axis_size("ep")
    capacity = 5 * row_count * TOP_K // (4 * expert_count)
    token_rows = moe_input.astype(jnp.float32)
    inverse = lax.rsqrt(jnp.mean(token_rows * token_rows, axis=1, keepdims=True) + eps)
    normed = (token_rows * inverse * moe_gain).astype(jnp.bfloat16)
    flat_ids = routes.reshape(-1)
    pair_count = flat_ids.shape[0]
    one_hot = (flat_ids[:, None] == jnp.arange(expert_count, dtype=jnp.int32)[None, :]).astype(
        jnp.int32
    )
    earlier_count = jnp.cumsum(one_hot, axis=0) - one_hot
    ranks = jnp.sum(earlier_count * one_hot, axis=1)
    slot_ids = flat_ids * capacity + ranks
    owners = (
        jnp.zeros((expert_count * capacity,), jnp.int32)
        .at[slot_ids]
        .set(jnp.arange(pair_count, dtype=jnp.int32) // TOP_K)
    )
    filled = (
        jnp.zeros((expert_count * capacity,), jnp.bfloat16)
        .at[slot_ids]
        .set(jnp.ones((pair_count,), jnp.bfloat16))
    )
    outgoing = normed[owners] * filled[:, None]
    w_gate = w_exp_gate[0]
    w_up = w_exp_up[0]
    w_down = w_exp_down[0]
    width = normed.shape[1] // lax.axis_size("tp")
    own_slice = lax.dynamic_slice_in_dim(outgoing, lax.axis_index("tp") * width, width, 1)
    arrived = lax.all_to_all(own_slice, "ep", split_axis=0, concat_axis=0, tiled=True)
    portion = lax.all_gather(arrived, "tp", axis=1, tiled=True)
    gate_sum = jnp.dot(portion, w_gate, preferred_element_type=jnp.float32)
    up_sum = jnp.dot(portion, w_up, preferred_element_type=jnp.float32)
    hidden = (jax.nn.silu(gate_sum) * up_sum).astype(jnp.bfloat16)
    partial_value = jnp.dot(hidden, w_down, preferred_element_type=jnp.float32)
    summed = lax.psum_scatter(
        partial_value.astype(jnp.bfloat16), "tp", scatter_dimension=1, tiled=True
    )
    returned = lax.all_to_all(summed, "ep", split_axis=0, concat_axis=0, tiled=True)
    picked = returned[slot_ids].astype(jnp.float32).reshape(row_count, TOP_K, returned.shape[1])
    combined = jnp.sum(picked * route_weight[:, :, None], axis=1)
    return combined.astype(jnp.bfloat16)


def body(
    mix_query,
    forget_input,
    mix_value,
    out_gate_input,
    decay_shift,
    forget_floor,
    head_gain,
    w_mix_out,
    moe_input,
    moe_gain,
    routes,
    route_weight,
    w_exp_gate,
    w_exp_up,
    w_exp_down,
):
    mixed = token_mixer(
        mix_query,
        forget_input,
        mix_value,
        out_gate_input,
        decay_shift,
        forget_floor,
        head_gain,
        w_mix_out,
    )
    moe_out = experts_layer(
        moe_input, moe_gain, routes, route_weight, w_exp_gate, w_exp_up, w_exp_down
    )
    return (mixed, moe_out)


def solution(mesh):
    placed = (
        P("ep", "tp"),
        P("ep", "tp"),
        P("ep", "tp"),
        P("ep", "tp"),
        P("ep", "tp"),
        P("tp"),
        P(),
        P(None, "tp"),
        P("ep", None),
        P(),
        P("ep", None),
        P("ep", None),
        P("ep", None, "tp"),
        P("ep", None, "tp"),
        P("ep", "tp", None),
    )
    return jax.shard_map(
        body, mesh=mesh, in_specs=placed, out_specs=(P("ep", "tp"), P("ep", "tp")), check_vma=False
    )
```

profile of v0, /device:TPU:0, one launch (start us, length us, event | category | flops | bytes accessed | tf_op | source)
XLA Modules:
  0.0 189.2 jit_solution(8927491651452208620)
XLA Ops:
  11.0 2.4 %scatter_custom_fusion = s32[640]{0:T(1024)S(1)} fusion(s32[512]{0:T(512)S(1)} %bitcast.123, s32[512]{0:T(512)S(1)} %add_select_fusion, s32[]{:T(128)} %constant.68.clone.1), kind=kCustom, calls=%fused_computation.82 | custom fusion | bytes 2564 | tf_op jit(solution)/shard_map/scatter | solution.py:114
  13.5 1.5 fusion.9
  15.0 1.5 fusion.11
  16.5 4.1 %gather_fusion = bf16[640,2048]{1,0:T(8,128)(2,1)} fusion(bf16[256,2048]{1,0:T(8,128)(2,1)S(1)} %fusion.11, s32[1024]{0:T(1024)S(1)} %pad_clamp_fusion.1), kind=kCustom, calls=%fused_computation | custom fusion | bytes 5245440 | tf_op jit(solution)/shard_map/gather | solution.py:121
  20.6 3.8 %scatter_custom_fusion.1 = bf16[640]{0:T(1024)(128)(2,1)S(1)} fusion(s32[512]{0:T(512)S(1)} %bitcast.124, bf16[512]{0:T(512)(128)(2,1)S(1)} %broadcast.119, bf16[]{:T(256)} %constant.79.clone.1), kind=kCustom, calls=%fused_computation.87 | custom fusion | bytes 1282 | tf_op jit(solution)/shard_map/scatter | solution.py:119
  24.4 1.3 dynamic-slice_multiply_fusion
  25.7 24.9 %all_to_all.24 = bf16[8,80,512]{2,1,0:T(8,128)(2,1)} all-to-all(bf16[8,80,512]{2,1,0:T(8,128)(2,1)S(1)} %bitcast.112), channel_id=1, replica_groups=mesh['ep'=8,'tp'=4] {'ep'}, dimensions={0} | all-to-all | bytes 1310720 | tf_op jit(solution)/shard_map/all_to_all | solution.py:127
  53.9 2.2 %copy.97 = f32[256,4,128]{2,1,0:T(4,128)} copy(f32[256,4,128]{0,2,1:T(8,128)} %bitcast.114) | data formatting | bytes 1048576 | tf_op jit(solution)/shard_map/reshape | solution.py:56
  58.8 2.8 %bitcast_multiply_fusion.2 = (f32[4,256,128]{2,0,1:T(4,128)}, f32[4,256,128]{2,0,1:T(4,128)S(1)}, f32[4,256,128]{2,0,1:T(4,128)S(1)}) fusion(f32[256,4,128]{2,1,0:T(4,128)} %copy.97, f32[4,128,256]{1,2,0:T(8,128)S(1)} %bitcast.110, f32[4,128]{1,0:T(4,128)S(1)} %get-tuple-element.60, f32[256,4,128]{2,1,0:T(4,128)} %copy.91), kind=kLoop, calls=%fused_computation.47 | loop fusion | flops 655360 | bytes 3147776 | tf_op jit(solution)/shard_map/mul | solution.py:63
  61.5 1.3 convolution_convert_fusion.1
  63.1 11.9 %all-gather.8.cloned.1.call-done = bf16[640,2048]{1,0:T(8,128)(2,1)} async-done(((bf16[640,512]{1,0:T(8,128)(2,1)}), bf16[640,2048]{1,0:T(8,128)(2,1)}) %all-gather.8.cloned.1.call-update) | async-done | bytes 2621456 | tf_op jit(solution)/shard_map/all_gather | solution.py:128
  75.0 7.4 %fusion.2 = f32[640,1024]{1,0:T(8,128)} fusion(bf16[640,2048]{1,0:T(8,128)(2,1)} %all-gather.8.cloned.1.call-done, bf16[1,2048,1024]{2,1,0:T(8,128)(2,1)} %param.30), kind=kOutput, calls=%fused_computation.8 | convolution fusion | flops 2684354560 | bytes 9437184 | tf_op jit(solution)/shard_map/dot_general | solution.py:130
  82.3 12.5 %fusion.6 = bf16[640,2048]{1,0:T(8,128)(2,1)} fusion(bf16[1,1024,2048]{2,1,0:T(8,128)(2,1)} %param.31, f32[640,1024]{1,0:T(8,128)} %fusion.2, bf16[640,2048]{1,0:T(8,128)(2,1)} %all-gather.8.cloned.1.call-done, bf16[1,2048,1024]{2,1,0:T(8,128)(2,1)} %param.29), kind=kOutput, calls=%fused_computation.12 | convolution fusion | flops 5373952000 | bytes 16252928 | tf_op jit(solution)/shard_map/dot_general | solution.py:132
  94.9 26.4 %all-gather = bf16[32,1,128]{2,1,0:T(2,128)(2,1)S(1)} all-gather(bf16[4,1,128]{2,1,0:T(2,128)(2,1)S(1)} %copy.102), channel_id=2, replica_groups=mesh['ep'=8,'tp'=4] {'ep'}, dimensions={0}, use_global_device_ids=true | all-gather | bytes 9216 | tf_op jit(solution)/shard_map/all_gather | solution.py:16
  121.6 3.0 %convolution_select_fusion = f32[4,256,256]{2,1,0:T(8,128)} fusion(f32[4,256,128]{2,0,1:T(4,128)} %get-tuple-element.57, pred[256,256]{1,0:T(8,128)(4,1)S(1)} %iota_compare_fusion, f32[4,256,128]{2,0,1:T(4,128)S(1)} %get-tuple-element.59), kind=kOutput, calls=%fused_computation.19 | convolution fusion | flops 402915328 | bytes 2162688 | tf_op jit(solution)/shard_map/htk,hsk->hts/dot_general | solution.py:62
  125.4 2.2 %multiply_reduce_fusion.1 = (f32[4,256]{1,0:T(4,128)S(1)}, f32[4,256,128]{1,2,0:T(8,128)S(1)}) fusion(f32[4,256,128]{1,2,0:T(8,128)S(1)} %fusion.36, f32[4,256,256]{2,1,0:T(8,128)} %convolution_select_fusion, bf16[256,512]{1,0:T(8,128)(2,1)} %param.19), kind=kOutput, calls=%fused_computation.54 | convolution fusion | flops 403045376 | bytes 2363392 | tf_op jit(solution)/shard_map/hts,hsv->htv/dot_general | solution.py:67
  128.4 25.2 %reduce-scatter.2.cloned.1.call-done = bf16[640,512]{1,0:T(8,128)(2,1)} async-done(((bf16[640,2048]{1,0:T(8,128)(2,1)}), bf16[640,512]{1,0:T(8,128)(2,1)}) %reduce-scatter.2.cloned.1.call-update) | async-done | bytes 655376 | tf_op jit(solution)/shard_map/reduce_scatter | solution.py:133
  153.7 5.5 %all-to-all-start.1 = ((bf16[8,80,512]{2,1,0:T(8,128)(2,1)}), bf16[8,80,512]{2,1,0:T(8,128)(2,1)S(1)}, u32[]{:S(2)}, u32[]{:S(2)}) async-start(bf16[8,80,512]{2,1,0:T(8,128)(2,1)} %bitcast.119), calls=%async_computation.2 | async-start | bytes 1310720 | tf_op jit(solution)/shard_map/all_to_all | solution.py:136
  159.3 13.1 %all-gather.6.cloned.1.call-done = bf16[256,2048]{0,1:T(8,128)(2,1)} async-done(((bf16[256,512]{0,1:T(8,128)(2,1)}), bf16[256,2048]{0,1:T(8,128)(2,1)}) %all-gather.6.cloned.1.call-update) | async-done | bytes 1048592 | tf_op jit(solution)/shard_map/all_gather | solution.py:89
  172.4 2.7 %convolution_convert_fusion = bf16[256,512]{1,0:T(8,128)(2,1)} fusion(bf16[256,2048]{0,1:T(8,128)(2,1)} %all-gather.6.cloned.1.call-done, bf16[2048,512]{1,0:T(8,128)(2,1)S(1)} %copy-done), kind=kOutput, calls=%fused_computation.21 | convolution fusion | flops 537001984 | bytes 3407872 | tf_op jit(solution)/shard_map/dot_general | solution.py:88
  175.0 1.3 all-to-all-done.1
  176.3 2.6 %gather_fusion.1 = bf16[512,512]{1,0:T(8,128)(2,1)} fusion(bf16[640,512]{1,0:T(8,128)(2,1)S(1)} %bitcast.108, s32[1024]{0:T(1024)S(1)} %pad_clamp_fusion), kind=kCustom, calls=%fused_computation.1 | custom fusion | bytes 1050624 | tf_op jit(solution)/shard_map/gather | solution.py:137
  178.9 1.7 reshape.158
  180.6 2.1 %multiply_reduce_fusion = bf16[256,512]{1,0:T(8,128)(2,1)} fusion(f32[256,2,512]{2,1,0:T(2,128)S(1)} %reshape.158, f32[256,2]{1,0:T(8,128)S(1)} %copy.110), kind=kLoop, calls=%fused_computation.23 | loop fusion | flops 393216 | bytes 1312768 | tf_op jit(solution)/shard_map/reduce_sum | solution.py:138
  (69 shorter events, 12.1 us)
Async XLA Ops:
  7.2 165.2 %copy-start = (bf16[2048,512]{1,0:T(8,128)(2,1)S(1)}, bf16[2048,512]{1,0:T(8,128)(2,1)}, u32[]{:S(2)}) copy-start(bf16[2048,512]{1,0:T(8,128)(2,1)} %param.24) | copy-start | bytes 6291460
  7.2 67.8 %all-gather.8.cloned.1.call-start = ((), (), s32[]{:S(2)}) async-start(), calls=%async_computation.4 | async-start | bytes 3276800 | tf_op jit(solution)/shard_map/all_gather | solution.py:128
  20.6 30.0 %copy-start.2 = (bf16[256,512]{1,0:T(8,128)(2,1)S(1)}, bf16[256,512]{1,0:T(8,128)(2,1)}, u32[]{:S(2)}) copy-start(bf16[256,512]{1,0:T(8,128)(2,1)} %param.18) | copy-start | bytes 786436
  20.6 30.2 %copy-start.4 = (f32[512]{0:T(512)S(1)}, f32[512]{0:T(512)}, u32[]{:S(2)}) copy-start(f32[512]{0:T(512)} %param.22) | copy-start | bytes 6148
  20.6 30.2 %copy-start.5 = (f32[256,4]{0,1:T(4,128)S(1)}, f32[256,4]{0,1:T(4,128)}, u32[]{:S(2)}) copy-start(f32[256,4]{0,1:T(4,128)} %param.21) | copy-start | bytes 12292
  50.6 74.1 %all-gather.10.cloned.1.call-start = ((), (), s32[]{:S(2)}) async-start(), calls=%async_computation.6 | async-start | bytes 1179648 | tf_op jit(solution)/shard_map/all_gather | solution.py:16
  53.9 7.6 %copy-start.1 = (bf16[256,512]{1,0:T(8,128)(2,1)S(1)}, bf16[256,512]{1,0:T(8,128)(2,1)}, u32[]{:S(2)}) copy-start(bf16[256,512]{1,0:T(8,128)(2,1)} %param.19) | copy-start | bytes 786436
  62.9 90.8 %reduce-scatter.2.cloned.1.call-start = ((), (), s32[]{:S(2)}) async-start(), calls=%async_computation.5 | async-start | bytes 3276800 | tf_op jit(solution)/shard_map/reduce_scatter | solution.py:133
  94.8 26.5 %copy-start.3 = (bf16[256,512]{1,0:T(8,128)(2,1)S(1)}, bf16[256,512]{1,0:T(8,128)(2,1)}, u32[]{:S(2)}) copy-start(bf16[256,512]{1,0:T(8,128)(2,1)} %param.20) | copy-start | bytes 786436
  94.8 77.6 %all-gather.6.cloned.1.call-start = ((), (), s32[]{:S(2)}) async-start(), calls=%async_computation.3 | async-start | bytes 1310720 | tf_op jit(solution)/shard_map/all_gather | solution.py:89
  124.7 2.9 %copy-start.7 = (f32[128]{0:T(128)S(1)}, f32[128]{0:T(128)}, u32[]{:S(2)}) copy-start(f32[128]{0:T(128)} %param.23) | copy-start | bytes 1540
  125.4 33.8 %copy-start.6 = (f32[256,2]{0,1:T(2,128)S(1)}, f32[256,2]{0,1:T(2,128)}, u32[]{:S(2)}) copy-start(f32[256,2]{0,1:T(2,128)} %param.28) | copy-start | bytes 6148
  153.7 22.6 %all-to-all-start.1 = ((bf16[8,80,512]{2,1,0:T(8,128)(2,1)}), bf16[8,80,512]{2,1,0:T(8,128)(2,1)S(1)}, u32[]{:S(2)}, u32[]{:S(2)}) async-start(bf16[8,80,512]{2,1,0:T(8,128)(2,1)} %bitcast.119), calls=%async_computation.2 | async-start | bytes 1310720 | tf_op jit(solution)/shard_map/all_to_all | solution.py:136
Sparse Core Ops, SparseCore 0:
  50.7 24.2 all-gather.7
  77.7 40.3 all-gather.9
  120.5 33.0 reduce-scatter.1
  155.7 16.6 all-gather.5
where the time goes:
time: 190 us; the launch traced here: 189 us
  waiting for transfers between devices  51.5 us (27%)
  blocking collectives  51.3 us (27%)
  matrix products  29.7 us (16%)
  local copies, waits for them, and re-layouts  22.4 us (12%)
  other arithmetic  14.5 us (8%)
  between operations  14 us (7%)
  starting transfers between devices  5.83 us (3%)
    all_gather x1, blocking collectives, carried_in(): lax.all_gather(a.astype(kind), axis)  26.4 us
    reduce_scatter x1, waiting for transfers between devices, experts_layer(): lax.psum_scatter(partial_value.astype(jnp.bfloat16), 'tp', scatter_dimens...  25.2 us
    all_to_all x1, blocking collectives, experts_layer(): lax.all_to_all(own_slice, 'ep', split_axis=0, concat_axis=0, tiled=True)  24.9 us
    all_gather x1, waiting for transfers between devices, token_mixer(): lax.all_gather(head_out, 'tp', axis=1, tiled=True)  13.1 us
    dot_general x1, matrix products, experts_layer(): partial_value = jnp.dot(hidden, w_down, preferred_element_type=jnp.float32)  12.5 us
    all_gather x1, waiting for transfers between devices, experts_layer(): portion = lax.all_gather(arrived, 'tp', axis=1, tiled=True)  11.9 us
    dot_general x1, matrix products, experts_layer(): up_sum = jnp.dot(portion, w_up, preferred_element_type=jnp.float32)  7.36 us
    all_to_all x1, starting transfers between devices, experts_layer(): lax.all_to_all(summed, 'ep', split_axis=0, concat_axis=0, tiled=True)  5.49 us
  transfers between devices with their start and end apart: 5, of which 4 were waited for; matrix products, arithmetic and copies ran while one was open for 22% of the time, Pallas kernels for 0%

commit v1 on v0

v1 whole, which is shorter than its diff:
```python
import functools

import jax
import jax.numpy as jnp
from jax import lax
from jax.experimental import pallas as pl
from jax.experimental.pallas import tpu as pltpu
from jax.sharding import PartitionSpec as P

TOP_K = 2
EPS = 1e-06
MESH = pl.DeviceIdType.MESH
BF = jnp.bfloat16
F32 = jnp.float32
HIGH = lax.Precision.HIGHEST


def mm(a, b, dims=((1,), (0,)), precision=None):
    return lax.dot_general(
        a, b, (dims, ((), ())), preferred_element_type=F32, precision=precision
    )


def scan_windows(ep):
    windows = [0]
    w = 1
    while w < ep - 1:
        windows.append(w)
        w *= 2
    return windows


def kernel(
    cfg,
    q_ref,
    fi_ref,
    v_ref,
    og_ref,
    ds_ref,
    ff_ref,
    hg_ref,
    x_ref,
    mg_ref,
    rt_ref,
    rw_ref,
    wm_hbm,
    wg_hbm,
    wu_hbm,
    wd_hbm,
    mixed_ref,
    moe_ref,
    wm,
    wg,
    wu,
    wd,
    disp,
    xs,
    hid,
    snd_p,
    rs_p,
    own,
    snd_y,
    rs_y,
    fin,
    ret,
    pick,
    ks_s,
    ks_r,
    carry,
    intra,
    qdec,
    ho,
    w_sem,
    a_ss,
    a_rs,
    gy_ss,
    gy_rs,
    gp_ss,
    gp_rs,
    rp_ss,
    rp_rs,
    ry_ss,
    ry_rs,
    b_ss,
    b_rs,
    k_ss,
    k_rs,
    hy_ss,
    hy_rs,
    hp_ss,
    hp_rs,
):
    ep, tp, cap, groups = cfg
    gb = ep // groups
    ny = tp // 2
    me = lax.axis_index("ep")
    t = lax.axis_index("tp")
    y = t // 2
    c = t % 2
    mate = y * 2 + (1 - c)
    rows, dim = x_ref.shape
    width = dim // tp
    slots = ep * cap
    hidden_units = wg.shape[1]
    heads = ds_ref.shape[1]
    hs = hg_ref.shape[1]
    hw = q_ref.shape[1]

    def ring(a, n):
        return lax.rem(a + n, n)

    def up_y(dy):
        return ring(y + dy, ny)

    def dn_y(dy):
        return ring(y - dy, ny)

    def rc(src, dst, ss, rs, e, j):
        return pltpu.make_async_remote_copy(
            src_ref=src, dst_ref=dst, send_sem=ss, recv_sem=rs, device_id=(e, j), device_id_type=MESH
        )

    loads = [
        pltpu.make_async_copy(wg_hbm.at[0], wg, w_sem.at[0]),
        pltpu.make_async_copy(wu_hbm.at[0], wu, w_sem.at[1]),
        pltpu.make_async_copy(wd_hbm.at[0], wd, w_sem.at[2]),
        pltpu.make_async_copy(wm_hbm, wm, w_sem.at[3]),
    ]
    barrier = pltpu.get_barrier_semaphore()
    for d in range(1, ep):
        pl.semaphore_signal(barrier, inc=1, device_id=(ring(me + d, ep), t), device_id_type=MESH)
    for dy in range(1, ny):
        pl.semaphore_signal(barrier, inc=1, device_id=(me, up_y(dy) * 2 + c), device_id_type=MESH)
    pl.semaphore_signal(barrier, inc=1, device_id=(me, mate), device_id_type=MESH)
    for load in loads:
        load.start()

    i_r = lax.broadcasted_iota(jnp.int32, (rows, rows), 0)
    i_c = lax.broadcasted_iota(jnp.int32, (rows, rows), 1)
    lane = lax.broadcasted_iota(jnp.int32, (rows, 128), 1)
    slot_lane = lax.broadcasted_iota(jnp.int32, (rows, slots), 1)
    rel, hot = [], []
    for k in range(TOP_K):
        e = rt_ref[:, k : k + 1]
        r = jnp.where(e >= me, e - me, e - me + ep)
        rel.append(r)
        hot.append((lane == r).astype(F32))
    before = mm((i_r > i_c).astype(F32).astype(BF), sum(hot).astype(BF))
    both = None
    for k in range(TOP_K):
        rank = jnp.sum(before * hot[k], axis=1, keepdims=True).astype(jnp.int32)
        p = (slot_lane == rel[k] * cap + rank).astype(F32)
        both = p if both is None else both + p
        pick[k] = p.astype(BF)
    xf = x_ref[...].astype(F32)
    inv = lax.rsqrt(jnp.mean(xf * xf, axis=1, keepdims=True) + EPS)
    cols = pl.ds(pl.multiple_of(t * width, width), width)
    normed = (x_ref[:, cols].astype(F32) * inv * mg_ref[:, cols]).astype(BF)
    out = mm(both.astype(BF), normed, ((0,), (0,))).astype(BF).reshape(ep, cap, width)
    disp[...] = out
    xs[t, 0] = out[0]

    pl.semaphore_wait(barrier, ep - 1 + ny)

    def a2a(d):
        return rc(disp.at[d], xs.at[t, d], a_ss.at[d], a_rs.at[d], ring(me + d, ep), t)

    for d in range(1, ep):
        a2a(d).start()

    def gat(col, g):
        return xs.at[col, pl.ds(g * gb, gb)]

    def gat_y(g, dy):
        r = gat(t, g)
        return rc(r, r, gy_ss.at[g, dy], gy_rs.at[g, dy], me, up_y(dy) * 2 + c)

    def gat_y_in(g, dy):
        r = gat(dn_y(dy) * 2 + c, g)
        return rc(r, r, gy_ss.at[g, dy], gy_rs.at[g, dy], me, mate)

    def gat_p(g, dy):
        r = gat(dn_y(dy) * 2 + c, g)
        return rc(r, r, gp_ss.at[g, dy], gp_rs.at[g, dy], me, mate)

    def gat_p_in(g, dy):
        r = gat(dn_y(dy) * 2 + 1 - c, g)
        return rc(r, r, gp_ss.at[g, dy], gp_rs.at[g, dy], me, mate)

    def relay1(g):
        for d in range(max(1, g * gb), (g + 1) * gb):
            a2a(d).wait_recv()
        for dy in range(1, ny):
            gat_y(g, dy).start()
        gat_p(g, 0).start()

    def relay2(g):
        for dy in range(1, ny):
            gat_y_in(g, dy).wait_recv()
            gat_p(g, dy).start()

    def arrived(g):
        for dy in range(ny):
            gat_p_in(g, dy).wait_recv()

    causal = i_r >= i_c
    tri = causal.astype(F32)

    def mix_all_decay():
        fl = ff_ref[...]
        fx = fi_ref[...].astype(F32)
        forget = fl + (1.0 - fl) * jax.nn.sigmoid(fx)
        return mm(tri, jnp.log(forget), precision=HIGH)

    def mix_head(h, run, s_col, s_row):
        hc = slice(h * hs, (h + 1) * hs)
        lr = run[:, hc]
        sc = s_col[:, h : h + 1]
        sr = s_row[h : h + 1, :]
        key = (1.0 - ff_ref[:, hc]) * jax.nn.sigmoid(-fi_ref[:, hc].astype(F32))
        q = q_ref[:, hc].astype(F32) * jnp.exp(lr)
        v = v_ref[:, hc]
        scores = mm(q.astype(BF), (key * jnp.exp(-lr)).astype(BF), ((1,), (1,)))
        scores = jnp.where(causal, scores * jnp.exp(jnp.minimum(sc - sr, 0.0)), 0.0)
        intra[:, hc] = mm(scores.astype(BF), v)
        qdec[:, hc] = (q * jnp.exp(sc)).astype(BF)
        l_end = lr[rows - 1 : rows, :]
        s_end = sc[rows - 1 : rows, :]
        kd = (key * jnp.exp(l_end - lr + (s_end - sc))).astype(BF)
        ks_s[0, h, 0:hs, :] = mm(v, kd, ((0,), (0,))).astype(BF)
        ks_s[0, h, hs : hs + 16, :] = jnp.broadcast_to(jnp.exp(l_end + s_end), (16, hs)).astype(BF)

    windows = scan_windows(ep)

    def scan_copy(i):
        hop = max(1, windows[i])
        return rc(ks_s.at[i], ks_r.at[i], k_ss.at[i], k_rs.at[i], ring(me + hop, ep), t)

    def scan_take(i):
        scan_copy(i).wait_recv()
        hop = max(1, windows[i])
        have = me >= hop
        for h in range(heads):
            got = ks_r[i, h].astype(F32)
            s_in = jnp.where(have, got[0:hs], 0.0)
            a_in = jnp.where(have, got[hs : hs + 16], 1.0)
            if i > 0:
                a_own = carry[h, hs : hs + 16, :]
                s_in = a_own[0:1] * s_in + carry[h, 0:hs, :]
                a_in = a_own * a_in
            carry[h, 0:hs, :] = s_in
            carry[h, hs : hs + 16, :] = a_in
            if i + 1 < len(windows):
                ks_s[i + 1, h, 0:hs, :] = s_in.astype(BF)
                ks_s[i + 1, h, hs : hs + 16, :] = a_in.astype(BF)
        if i + 1 < len(windows):
            scan_copy(i + 1).start()

    def ho_y(dy):
        return rc(ho.at[t], ho.at[t], hy_ss.at[dy], hy_rs.at[dy], me, up_y(dy) * 2 + c)

    def ho_y_in(dy):
        r = ho.at[dn_y(dy) * 2 + c]
        return rc(r, r, hy_ss.at[dy], hy_rs.at[dy], me, mate)

    def ho_p(dy):
        r = ho.at[dn_y(dy) * 2 + c]
        return rc(r, r, hp_ss.at[dy], hp_rs.at[dy], me, mate)

    def ho_p_in(dy):
        r = ho.at[dn_y(dy) * 2 + 1 - c]
        return rc(r, r, hp_ss.at[dy], hp_rs.at[dy], me, mate)

    def mix_close():
        for h in range(heads):
            hc = slice(h * hs, (h + 1) * hs)
            o = intra[:, hc] + mm(qdec[:, hc], carry[h, 0:hs, :].astype(BF), ((1,), (1,)))
            iv = lax.rsqrt(jnp.mean(o * o, axis=1, keepdims=True) + EPS)
            g = og_ref[:, hc].astype(F32)
            ho[t, :, hc] = (o * iv * hg_ref[...] * (g * jax.nn.sigmoid(g))).astype(BF)
        for dy in range(1, ny):
            ho_y(dy).start()
        ho_p(0).start()

    def ho_relay():
        for dy in range(1, ny):
            ho_y_in(dy).wait_recv()
            ho_p(dy).start()

    gr = gb * cap
    ft = min(256, hidden_units)

    def first(g):
        def tile(n, _):
            fc = pl.ds(pl.multiple_of(n * ft, ft), ft)
            gate = jnp.zeros((gr, ft), F32)
            up = jnp.zeros((gr, ft), F32)
            for j in range(tp):
                a = xs[j, g * gb : (g + 1) * gb].reshape(gr, width)
                gate += mm(a, wg[j * width : (j + 1) * width, fc])
                up += mm(a, wu[j * width : (j + 1) * width, fc])
            hid[:, fc] = (gate * jax.nn.sigmoid(gate) * up).astype(BF)
            return 0

        lax.fori_loop(0, hidden_units // ft, tile, 0)

    def down(dy, core):
        col = up_y(dy) * 2 + core
        return mm(hid[...], wd[:, pl.ds(pl.multiple_of(col * width, width), width)])

    def red_p(g, dy):
        return rc(snd_p.at[g, dy], rs_p.at[g, dy], rp_ss.at[g, dy], rp_rs.at[g, dy], me, mate)

    def red_y(g, dy):
        return rc(
            snd_y.at[g, dy], rs_y.at[g, dy], ry_ss.at[g, dy], ry_rs.at[g, dy], me, up_y(dy) * 2 + c
        )

    order = list(range(1, ny)) + [0]

    def second(g):
        for dy in order:
            snd_p[g, dy] = down(dy, 1 - c).astype(BF)
            red_p(g, dy).start()
        for dy in order:
            own[g % 2, dy] = down(dy, c)
        for dy in order:
            red_p(g, dy).wait_recv()
            total = own[g % 2, dy] + rs_p[g, dy].astype(F32)
            if dy:
                snd_y[g, dy] = total.astype(BF)
                red_y(g, dy).start()
            else:
                own[g % 2, 0] = total

    def back(d):
        return rc(fin.at[d], ret.at[d], b_ss.at[d], b_rs.at[d], ring(me - d, ep), t)

    def third(g):
        total = own[g % 2, 0]
        for dy in range(1, ny):
            red_y(g, dy).wait_recv()
            total += rs_y[g, dy].astype(F32)
        blocks = total.astype(BF).reshape(gb, cap, width)
        for i in range(gb):
            d = g * gb + i
            if d == 0:
                ret[0] = blocks[0]
            else:
                fin[d] = blocks[i]
                back(d).start()

    run = mix_all_decay()
    s_col = mm(tri, ds_ref[...], precision=HIGH)
    s_row = mm(ds_ref[...], (i_r <= i_c).astype(F32), ((0,), (0,)), precision=HIGH)
    for h in range(heads):
        mix_head(h, run, s_col, s_row)
        if h == heads // 2:
            relay1(0)
    scan_copy(0).start()
    relay1(1)
    relay2(0)
    scan_take(0)
    relay1(2)
    for load in loads[:3]:
        load.wait()
    taken = 1
    for g in range(groups):
        arrived(g)
        first(g)
        if g + 1 < groups:
            relay2(g + 1)
        if g + 3 < groups:
            relay1(g + 3)
        second(g)
        if taken < len(windows):
            scan_take(taken)
            taken += 1
        if g > 0:
            third(g - 1)
    while taken < len(windows):
        scan_take(taken)
        taken += 1
    mix_close()
    third(groups - 1)
    ho_relay()
    loads[3].wait()
    for dy in range(ny):
        ho_p_in(dy).wait_recv()
    acc = jnp.zeros(mixed_ref.shape, F32)
    for j in range(tp):
        acc += mm(ho[j], wm[j * hw : (j + 1) * hw, :])
    mixed_ref[...] = acc.astype(BF)
    for d in range(1, ep):
        back(d).wait_recv()
    flat = ret[...].reshape(slots, width)
    res = jnp.zeros(moe_ref.shape, F32)
    for k in range(TOP_K):
        res += mm(pick[k], flat) * rw_ref[:, k : k + 1]
    moe_ref[...] = res.astype(BF)

    for d in range(1, ep):
        a2a(d).wait_send()
        back(d).wait_send()
    for i in range(len(windows)):
        scan_copy(i).wait_send()
    for dy in range(ny):
        ho_p(dy).wait_send()
        if dy:
            ho_y(dy).wait_send()
        for g in range(groups):
            gat_p(g, dy).wait_send()
            red_p(g, dy).wait_send()
            if dy:
                gat_y(g, dy).wait_send()
                red_y(g, dy).wait_send()


def body(ep, tp, *args):
    (q, fi, v, og, ds, ff, hg, wm, x, mg, rt, rw, wg, wu, wd) = args
    rows, dim = x.shape
    capacity = 5 * rows * TOP_K // (4 * ep)
    cap = -(-capacity // 16) * 16
    groups = 4
    gb = ep // groups
    ny = tp // 2
    width = dim // tp
    heads = ds.shape[1]
    hs = hg.shape[0]
    hw = q.shape[1]
    steps = len(scan_windows(ep))
    fu = wg.shape[2]
    gr = gb * cap
    vm = pltpu.VMEM
    dma = pltpu.SemaphoreType.DMA
    scratch = [
        vm(wm.shape, BF),
        vm(wg.shape[1:], BF),
        vm(wu.shape[1:], BF),
        vm(wd.shape[1:], BF),
        vm((ep, cap, width), BF),
        vm((tp, ep, cap, width), BF),
        vm((gr, fu), BF),
        vm((groups, ny, gr, width), BF),
        vm((groups, ny, gr, width), BF),
        vm((2, ny, gr, width), F32),
        vm((groups, ny, gr, width), BF),
        vm((groups, ny, gr, width), BF),
        vm((ep, cap, width), BF),
        vm((ep, cap, width), BF),
        vm((TOP_K, rows, ep * cap), BF),
        vm((steps, heads, hs + 16, hs), BF),
        vm((steps, heads, hs + 16, hs), BF),
        vm((heads, hs + 16, hs), F32),
        vm((rows, hw), F32),
        vm((rows, hw), BF),
        vm((tp, rows, hw), BF),
        dma((4,)),
        dma((ep,)),
        dma((ep,)),
        dma((groups, ny)),
        dma((groups, ny)),
        dma((groups, ny)),
        dma((groups, ny)),
        dma((groups, ny)),
        dma((groups, ny)),
        dma((groups, ny)),
        dma((groups, ny)),
        dma((ep,)),
        dma((ep,)),
        dma((steps,)),
        dma((steps,)),
        dma((ny,)),
        dma((ny,)),
        dma((ny,)),
        dma((ny,)),
    ]
    out = jax.ShapeDtypeStruct((rows, width), BF)
    in_vm = pl.BlockSpec(memory_space=pltpu.VMEM)
    in_any = pl.BlockSpec(memory_space=pl.ANY)
    return pl.pallas_call(
        functools.partial(kernel, (ep, tp, cap, groups)),
        out_shape=(out, out),
        in_specs=[in_vm] * 11 + [in_any] * 4,
        out_specs=(in_vm, in_vm),
        scratch_shapes=scratch,
        compiler_params=pltpu.CompilerParams(
            collective_id=0, has_side_effects=True, vmem_limit_bytes=60 * 1024 * 1024
        ),
    )(q, fi, v, og, ds, ff[None, :], hg[None, :], x, mg[None, :], rt, rw, wm, wg, wu, wd)


def solution(mesh):
    placed = (
        P("ep", "tp"),
        P("ep", "tp"),
        P("ep", "tp"),
        P("ep", "tp"),
        P("ep", "tp"),
        P("tp"),
        P(),
        P(None, "tp"),
        P("ep", None),
        P(),
        P("ep", None),
        P("ep", None),
        P("ep", None, "tp"),
        P("ep", None, "tp"),
        P("ep", "tp", None),
    )
    return jax.shard_map(
        functools.partial(body, mesh.shape["ep"], mesh.shape["tp"]),
        mesh=mesh,
        in_specs=placed,
        out_specs=(P("ep", "tp"), P("ep", "tp")),
        check_vma=False,
    )
```

time: 190 us -> 74.4 us (0.39)
  Pallas kernels: 0 us -> 65.1 us
  waiting for transfers between devices: 51.5 us -> 0 us
  blocking collectives: 51.3 us -> 0 us
  matrix products: 29.7 us -> 0 us
  local copies, waits for them, and re-layouts: 22.4 us -> 7.77 us
  other arithmetic: 14.5 us -> 0 us
  between operations: 14 us -> 0.64 us
  starting transfers between devices: 5.83 us -> 0 us
    pallas_call x0 -> x1, Pallas kernels: none -> 65.1 us  [body(): pl.pallas_call(functools.partial(kernel, (ep, tp, cap, groups)), out_shap...]
    dot_general x7 -> x0, matrix products: 29.7 us -> none  [the longest x1 12.5 us: experts_layer(): partial_value = jnp.dot(hidden, w_down, preferred_element_type=jnp.float32)]
    all_gather x1 -> x0, blocking collectives: 26.4 us -> none  [carried_in(): lax.all_gather(a.astype(kind), axis)]
    reduce_scatter x1 -> x0, waiting for transfers between devices: 25.2 us -> none  [experts_layer(): lax.psum_scatter(partial_value.astype(jnp.bfloat16), 'tp', scatter_dimens...]
    all_gather x3 -> x0, waiting for transfers between devices: 24.9 us -> none  [the longest x1 13.1 us: token_mixer(): lax.all_gather(head_out, 'tp', axis=1, tiled=True)]
    all_to_all x1 -> x0, blocking collectives: 24.9 us -> none  [experts_layer(): lax.all_to_all(own_slice, 'ep', split_axis=0, concat_axis=0, tiled=True)]
    gather x2 -> x0, local copies, waits for them, and re-layouts: 6.7 us -> none  [the longest x1 4.09 us: experts_layer(): outgoing = normed[owners] * filled[:, None]]
    scatter x2 -> x0, local copies, waits for them, and re-layouts: 6.21 us -> none  [the longest x1 3.77 us: experts_layer(): filled = jnp.zeros((expert_count * capacity,), jnp.bfloat16).at[slot_ids]...]
  transfers between devices with their start and end apart: 5 -> 0, of which waited for: 4 -> 0; matrix products, arithmetic and copies ran while one was open for 22% -> 0% of each run, Pallas kernels for 0% -> 0%
where the time goes in v1:
time: 74.4 us; the launch traced here: 73.5 us
  Pallas kernels  65.1 us (87%)
  local copies, waits for them, and re-layouts  7.77 us (10%)
    pallas_call x1, Pallas kernels, body(): pl.pallas_call(functools.partial(kernel, (ep, tp, cap, groups)), out_shap...  65.1 us
    unnamed x5, local copies, waits for them, and re-layouts  7.77 us

profile of v1, /device:TPU:0, one launch (start us, length us, event | category | flops | bytes accessed | tf_op | source)
XLA Modules:
  0.0 73.5 jit_solution(7573177846503933003)
XLA Ops:
  0.6 1.5 %copy.17.ds_ref = f32[256,4]{1,0:T(8,128)} copy(f32[256,4]{0,1:T(4,128)} %param.19) | data formatting | bytes 8192 | tf_op args[4]
  2.1 1.5 %copy.18.rt_ref = s32[256,2]{1,0:T(8,128)} copy(s32[256,2]{0,1:T(2,128)} %param.25) | data formatting | bytes 4096 | tf_op args[10]
  3.6 1.5 %copy.19.rw_ref = f32[256,2]{1,0:T(8,128)} copy(f32[256,2]{0,1:T(2,128)} %param.26) | data formatting | bytes 4096 | tf_op args[11]
  5.1 65.1 %shard_map.158 = (bf16[256,512]{1,0:T(8,128)(2,1)}, bf16[256,512]{1,0:T(8,128)(2,1)}) custom-call(bf16[256,512]{1,0:T(8,128)(2,1)} %q_ref.1, bf16[256,512]{1,0:T(8,128)(2,1)} %fi_ref.1, bf16[256,512]{1,0:T(8,128)(2,1)} %v_ref.1, bf16[256,512]{1,0:T(8,128)(2,1)} %og_ref.1, f32[256,4]{1,0:T(8,128)} %copy.17.ds_ref, f32[1,512]{1,0:T(1,128)} %bitcast.4, ...), custom_call_target="tpu_custom_call" | custom-call | tf_op jit(solution)/shard_map/pallas_call | solution.py:481
  70.2 1.7 %copy.22 = bf16[256,512]{1,0:T(8,128)(2,1)} copy(bf16[256,512]{1,0:T(8,128)(2,1)} %get-tuple-element.4) | data formatting | bytes 524288
  71.9 1.7 %copy.23 = bf16[256,512]{1,0:T(8,128)(2,1)} copy(bf16[256,512]{1,0:T(8,128)(2,1)} %get-tuple-element.5) | data formatting | bytes 524288

commit v2 on v1

--- a/solution.py
+++ b/solution.py
@@ -102,7 +102,7 @@
     width = dim // tp
     slots = ep * cap
     hidden_units = wg.shape[1]
-    heads = ds_ref.shape[1]
+    heads = ds_ref.shape[0]
     hs = hg_ref.shape[1]
     hw = q_ref.shape[1]
 
@@ -139,9 +139,11 @@
     i_c = lax.broadcasted_iota(jnp.int32, (rows, rows), 1)
     lane = lax.broadcasted_iota(jnp.int32, (rows, 128), 1)
     slot_lane = lax.broadcasted_iota(jnp.int32, (rows, slots), 1)
+    eye = (i_r == i_c).astype(F32)
+    ids = mm(eye, rt_ref[...].astype(F32), ((1,), (1,)), HIGH).astype(jnp.int32)
     rel, hot = [], []
     for k in range(TOP_K):
-        e = rt_ref[:, k : k + 1]
+        e = ids[:, k : k + 1]
         r = jnp.where(e >= me, e - me, e - me + ep)
         rel.append(r)
         hot.append((lane == r).astype(F32))
@@ -236,10 +238,18 @@
         hop = max(1, windows[i])
         return rc(ks_s.at[i], ks_r.at[i], k_ss.at[i], k_rs.at[i], ring(me + hop, ep), t)
 
+    def scan_send(i, act):
+        pl.when(me + max(1, windows[i]) < ep)(lambda: act(scan_copy(i)))
+
     def scan_take(i):
-        scan_copy(i).wait_recv()
         hop = max(1, windows[i])
         have = me >= hop
+
+        @pl.when(jnp.logical_not(have))
+        def _():
+            ks_r[i] = jnp.zeros(ks_r.shape[1:], BF)
+
+        pl.when(have)(lambda: scan_copy(i).wait_recv())
         for h in range(heads):
             got = ks_r[i, h].astype(F32)
             s_in = jnp.where(have, got[0:hs], 0.0)
@@ -254,7 +264,7 @@
                 ks_s[i + 1, h, 0:hs, :] = s_in.astype(BF)
                 ks_s[i + 1, h, hs : hs + 16, :] = a_in.astype(BF)
         if i + 1 < len(windows):
-            scan_copy(i + 1).start()
+            scan_send(i + 1, lambda a: a.start())
 
     def ho_y(dy):
         return rc(ho.at[t], ho.at[t], hy_ss.at[dy], hy_rs.at[dy], me, up_y(dy) * 2 + c)
@@ -351,13 +361,13 @@
                 back(d).start()
 
     run = mix_all_decay()
-    s_col = mm(tri, ds_ref[...], precision=HIGH)
-    s_row = mm(ds_ref[...], (i_r <= i_c).astype(F32), ((0,), (0,)), precision=HIGH)
+    s_col = mm(tri, ds_ref[...], ((1,), (1,)), HIGH)
+    s_row = mm(ds_ref[...], tri, ((1,), (1,)), HIGH)
     for h in range(heads):
         mix_head(h, run, s_col, s_row)
         if h == heads // 2:
             relay1(0)
-    scan_copy(0).start()
+    scan_send(0, lambda a: a.start())
     relay1(1)
     relay2(0)
     scan_take(0)
@@ -395,15 +405,16 @@
         back(d).wait_recv()
     flat = ret[...].reshape(slots, width)
     res = jnp.zeros(moe_ref.shape, F32)
+    weight = mm(eye, rw_ref[...], ((1,), (1,)), HIGH)
     for k in range(TOP_K):
-        res += mm(pick[k], flat) * rw_ref[:, k : k + 1]
+        res += mm(pick[k], flat) * weight[:, k : k + 1]
     moe_ref[...] = res.astype(BF)
 
     for d in range(1, ep):
         a2a(d).wait_send()
         back(d).wait_send()
     for i in range(len(windows)):
-        scan_copy(i).wait_send()
+        scan_send(i, lambda a: a.wait_send())
     for dy in range(ny):
         ho_p(dy).wait_send()
         if dy:
@@ -414,6 +425,11 @@
             if dy:
                 gat_y(g, dy).wait_send()
                 red_y(g, dy).wait_send()
+
+
+def emit(a_ref, b_ref, a_out, b_out):
+    a_out[...] = a_ref[...]
+    b_out[...] = b_ref[...]
 
 
 def body(ep, tp, *args):
@@ -478,7 +494,7 @@
     out = jax.ShapeDtypeStruct((rows, width), BF)
     in_vm = pl.BlockSpec(memory_space=pltpu.VMEM)
     in_any = pl.BlockSpec(memory_space=pl.ANY)
-    return pl.pallas_call(
+    made = pl.pallas_call(
         functools.partial(kernel, (ep, tp, cap, groups)),
         out_shape=(out, out),
         in_specs=[in_vm] * 11 + [in_any] * 4,
@@ -487,7 +503,10 @@
         compiler_params=pltpu.CompilerParams(
             collective_id=0, has_side_effects=True, vmem_limit_bytes=60 * 1024 * 1024
         ),
-    )(q, fi, v, og, ds, ff[None, :], hg[None, :], x, mg[None, :], rt, rw, wm, wg, wu, wd)
+    )(q, fi, v, og, ds.T, ff[None, :], hg[None, :], x, mg[None, :], rt.T, rw.T, wm, wg, wu, wd)
+    return pl.pallas_call(
+        emit, out_shape=(out, out), in_specs=[in_vm] * 2, out_specs=(in_vm, in_vm), name="emit"
+    )(*made)
 
 
 def solution(mesh):

time: 74.4 us -> 67.4 us (0.906)
  local copies, waits for them, and re-layouts: 7.77 us -> 0 us
  Pallas kernels: 65.1 us -> 66.3 us
    unnamed x5 -> x0, local copies, waits for them, and re-layouts: 7.77 us -> none
    pallas_call x0 -> x1, Pallas kernels: none -> 1.84 us  [body(): pl.pallas_call(emit, out_shape=(out, out), in_specs=[in_vm] * 2, out_spec...]
where the time goes in v2:
time: 67.4 us; the launch traced here: 67 us
  Pallas kernels  66.3 us (98%)
    pallas_call x1, Pallas kernels, body(): pl.pallas_call(functools.partial(kernel, (ep, tp, cap, groups)), out_shap...  64.5 us
    pallas_call x1, Pallas kernels, body(): pl.pallas_call(emit, out_shape=(out, out), in_specs=[in_vm] * 2, out_spec...  1.84 us

profile of v2, /device:TPU:0, one launch (start us, length us, event | category | flops | bytes accessed | tf_op | source)
XLA Modules:
  0.0 67.0 jit_solution(4461423724737441598)
XLA Ops:
  0.6 64.5 %shard_map.158 = (bf16[256,512]{1,0:T(8,128)(2,1)}, bf16[256,512]{1,0:T(8,128)(2,1)}) custom-call(bf16[256,512]{1,0:T(8,128)(2,1)} %q_ref.1, bf16[256,512]{1,0:T(8,128)(2,1)} %fi_ref.1, bf16[256,512]{1,0:T(8,128)(2,1)} %v_ref.1, bf16[256,512]{1,0:T(8,128)(2,1)} %og_ref.1, f32[4,256]{1,0:T(4,128)} %bitcast.7, f32[1,512]{1,0:T(1,128)} %bitcast.8, ...), custom_call_target="tpu_custom_call" | custom-call | tf_op jit(solution)/shard_map/pallas_call | solution.py:497
  65.1 1.8 %emit.1 = (bf16[256,512]{1,0:T(8,128)(2,1)}, bf16[256,512]{1,0:T(8,128)(2,1)}) custom-call(bf16[256,512]{1,0:T(8,128)(2,1)} %get-tuple-element.4.a_ref, bf16[256,512]{1,0:T(8,128)(2,1)} %get-tuple-element.5.b_ref), custom_call_target="tpu_custom_call" | custom-call | tf_op jit(solution)/shard_map/emit/pallas_call | solution.py:507
